TPU v7x, 32 devices: a whole 2x2x4 slice. The times are simulated.
32 devices in a mesh: ep: 4 (over y, x), tp: 8 (over z, core).
Axes of the slice: x: 2, y: 2, z: 4, core: 2. Of those that a mesh axis runs over, the one named last changes fastest.
Arguments:
- queries: bfloat16 [4096, 1024], P('ep', 'tp'), may hold values from -6 to 6
- keys: bfloat16 [4096, 256], P('ep'), may hold values from -6 to 6, as said below
- values: bfloat16 [4096, 256], P('ep'), may hold values from -6 to 6
- slopes: float32 [16], P('tp'), may hold values from 0.002 to 0.08
- sinks: float32 [16], P('tp'), may hold values from 2 to 6
- out_weight: bfloat16 [1024, 2048], P('tp'), may hold values from -0.1875 to 0.1875
- mix_gain: float32 [2048], replicated, may hold values from 0.1 to 1.9
- moe_input: bfloat16 [4096, 2048], P(('ep', 'tp')), may hold values from -6 to 6
- in_gain: float32 [2048], replicated, may hold values from 0.1 to 1.9
- out_gain: float32 [2048], replicated, may hold values from 0.1 to 1.9
- group_router: bfloat16 [2048, 4], replicated, may hold values from -0.125 to 0.125
- expert_router: bfloat16 [2048, 4], replicated, may hold values from -0.125 to 0.125
- routes: int32 [4096, 2], P(('ep', 'tp')), may hold values from 0 to 3, all different within a row; in each aligned block of 128 rows (0 to 127, 128 to 255, ...) at most 96 rows name the same one
- gate_weight: bfloat16 [4, 2048, 1024], P('ep', None, 'tp'), may hold values from -0.125 to 0.125
- up_weight: bfloat16 [4, 2048, 1024], P('ep', None, 'tp'), may hold values from -0.125 to 0.125
- down_weight: bfloat16 [4, 2048, 1024], P('ep', None, 'tp'), may hold values from -0.1875 to 0.1875
Outputs:
- mixer_output: bfloat16 [4096, 2048], P(('ep', 'tp'))
- moe_output: bfloat16 [4096, 2048], P(('ep', 'tp'))
Inputs may be any that keep to these rules, and one draw needn't show every extreme that they name: `keys`: keys share one value range with the queries. `routes`: A token names 2 different experts. Among the rows of one device no expert is named more than 96 times, a bound that some block reaches in every draw.
All inputs are finite; a program needn't handle non-finite values.
Results may differ from a plain program's by a relative error of at most 0.018.
Values may be sent and summed in bfloat16 or wider, within the bound.
A program may use at most 128 MiB of HBM per device.

v0:
```python
import functools
import math

import jax
import jax.numpy as jnp
from jax import lax
from jax.experimental import pallas as pl
from jax.experimental.pallas import tpu as pltpu
from jax.sharding import PartitionSpec as P

HEADS = 16
HD = 64
KV_HEADS = 4
WINDOW = 128
CHUNKS = 4


eps = 1e-06
MESH = pl.DeviceIdType.MESH
F32 = jnp.float32
BF16 = jnp.bfloat16


def flipped(index, bit):
    return index + bit - 2 * bit * ((index // bit) % 2)


def partner_of(index, offset, size):
    bit = 1
    while bit < size:
        if offset & bit:
            index = flipped(index, bit)
        bit *= 2
    return index


def bits_of(size):
    return [1 << i for i in range((size - 1).bit_length())]


def offsets_of(order):
    offsets = [0]
    for bit in order:
        offsets = offsets + [offset ^ bit for offset in offsets]
    return offsets


def scale_rows(matrix, gain):
    mean_square = jnp.mean(matrix * matrix, axis=-1, keepdims=True)
    return matrix * lax.rsqrt(mean_square + eps) * gain


def kernel(
    n_ep,
    n_tp,
    queries,
    keys,
    values,
    slopes,
    sinks,
    out_weight,
    mix_gain,
    moe_input,
    in_gain,
    out_gain,
    group_router,
    expert_router,
    routes,
    gate_weight,
    up_weight,
    down_weight,
    mixer_output,
    moe_output,
    gates,
    ups,
    downs,
    tokens,
    tables,
    key_rows,
    value_rows,
    attended,
    pieces,
    share,
    projected,
    hidden,
    landed,
    total,
    local_sem,
    ep_send,
    ep_recv,
    tp_send,
    tp_recv,
    rs_send,
    rs_recv,
):
    me_ep, me_tp = lax.axis_index("ep"), lax.axis_index("tp")
    rows, width = moe_input.shape
    local, _, units = gate_weight.shape
    group_rows = rows * n_tp
    columns = width // n_ep
    chunk = width // CHUNKS
    half_chunk = chunk // 2
    forth = bits_of(n_ep)
    back = forth[::-1]
    tp_order = bits_of(n_tp)[::-1]
    tp_offsets = offsets_of(tp_order)
    cut = group_rows_cut = share.shape[1] // 2

    sent = []
    locals_ = []

    def local_copy(source, target):
        copy = pltpu.make_async_copy(source, target, local_sem.at[len(locals_)])
        copy.start()
        locals_.append(copy)
        return copy

    def send(source, target, send_sem, recv_sem, where):
        copy = pltpu.make_async_remote_copy(
            src_ref=source,
            dst_ref=target,
            send_sem=send_sem,
            recv_sem=recv_sem,
            device_id=where,
            device_id_type=MESH,
        )
        copy.start()
        sent.append(copy)
        return copy

    class Spread:
        def __init__(self, number, own, slot_of, order):
            self.number, self.own, self.slot_of, self.order = number, own, slot_of, order
            self.coming = {}
            self.ready = {0}

        def post(self, source, offset, bit):
            target = offset ^ bit
            self.coming[target] = send(
                source,
                self.slot_of(target),
                ep_send.at[self.number, target],
                ep_recv.at[self.number, target],
                {"ep": flipped(me_ep, bit)},
            )

        def first(self, step):
            self.post(self.own, 0, self.order[step])

        def wait(self, offset):
            if offset not in self.ready:
                self.coming[offset].wait_recv()
                self.ready.add(offset)

        def forward(self):
            held = [0]
            for bit in self.order:
                for offset in held:
                    if offset:
                        self.wait(offset)
                        self.post(self.slot_of(offset), offset, bit)
                held = held + [offset ^ bit for offset in held]

    gate_spread = Spread(0, gate_weight, lambda o: gates.at[o], forth)
    up_spread = Spread(1, up_weight, lambda o: ups.at[o], back)
    down_spreads = []
    for c in range(CHUNKS):
        for part, order in ((0, forth), (1, back)):
            span = pl.ds(c * chunk + part * half_chunk, half_chunk)
            down_spreads.append(
                Spread(
                    2 + 2 * c + part,
                    down_weight.at[:, span],
                    lambda o, span=span: downs.at[o, :, span],
                    order,
                )
            )
    share_spreads = [
        Spread(
            2 + 2 * CHUNKS + part,
            share.at[0, pl.ds(part * cut, cut)],
            lambda o, part=part: share.at[o, pl.ds(part * cut, cut)],
            order,
        )
        for part, order in ((0, forth), (1, back))
    ]
    halo_number = 4 + 2 * CHUNKS

    take_keys = local_copy(keys, key_rows.at[pl.ds(WINDOW, group_rows)])
    take_values = local_copy(values, value_rows.at[pl.ds(WINDOW, group_rows)])
    take_gate = local_copy(gate_weight, gates.at[0])
    take_up = local_copy(up_weight, ups.at[0])
    take_down = local_copy(down_weight, downs.at[0])
    own_columns = pl.ds(pl.multiple_of(me_ep * columns, columns), columns)
    take_share = local_copy(out_weight.at[:, own_columns], share.at[0, pl.ds(0, out_weight.shape[0])])

    ep_next = lax.rem(me_ep + 1, n_ep)
    ep_prev = lax.rem(me_ep + n_ep - 1, n_ep)
    barrier = pltpu.get_barrier_semaphore()
    greeted = [{"tp": partner_of(me_tp, offset, n_tp)} for offset in range(1, n_tp)]
    greeted += [{"ep": flipped(me_ep, bit)} for bit in forth]
    greeted += [{"ep": ep_next}, {"ep": ep_prev}]
    for where in greeted:
        pl.semaphore_signal(barrier, inc=1, device_id=where, device_id_type=MESH)
    pl.semaphore_wait(barrier, len(greeted))

    halo = []
    last_rows = pl.ds(group_rows - WINDOW, WINDOW)
    for place, (source, target) in enumerate(((keys, key_rows), (values, value_rows))):
        halo.append(
            send(
                source.at[last_rows],
                target.at[pl.ds(0, WINDOW)],
                ep_send.at[halo_number + place, 0],
                ep_recv.at[halo_number + place, 0],
                {"ep": ep_next},
            )
        )
    for step in range(len(forth)):
        gate_spread.first(step)
        up_spread.first(step)

    normed = scale_rows(moe_input[...].astype(F32), in_gain[...]).astype(BF16)
    tokens[pl.ds(0, rows)] = normed
    coming = {}
    token_ready = {0}

    def span_of(position):
        return pl.ds(position * rows, rows)

    def token_send(position, step):
        target = position + (1 << step)
        coming[target] = send(
            tokens.at[span_of(position)],
            tokens.at[span_of(target)],
            tp_send.at[0, target],
            tp_recv.at[0, target],
            {"tp": flipped(me_tp, tp_order[step])},
        )

    def token_wait(position):
        if position not in token_ready:
            coming[position].wait_recv()
            token_ready.add(position)

    steps = len(tp_order)
    for step in reversed(range(steps)):
        token_send(0, step)

    def to_all(number, source_of, target_of):
        waits = []
        for position in range(1, n_tp):
            other = partner_of(me_tp, tp_offsets[position], n_tp)
            waits.append(
                send(
                    source_of(other),
                    target_of(position),
                    tp_send.at[number, position],
                    tp_recv.at[number, position],
                    {"tp": other},
                )
            )
        return waits

    group_logits = jnp.dot(normed, group_router[...], preferred_element_type=F32)
    expert_logits = jnp.dot(normed, expert_router[...], preferred_element_type=F32)
    experts, groups = expert_logits.shape[1], group_logits.shape[1]
    per_group = experts // groups
    group_shifted = jnp.exp(group_logits - jnp.max(group_logits, axis=-1, keepdims=True))
    group_prob = group_shifted / jnp.sum(group_shifted, axis=-1, keepdims=True)
    expert_ids = lax.broadcasted_iota(jnp.int32, (rows, experts), 1)
    group_ids = lax.broadcasted_iota(jnp.int32, (rows, groups), 1)
    visited = [routes[:, k : k + 1] for k in range(routes.shape[1])]
    matches = [expert_ids == visit for visit in visited]
    picked = [
        jnp.sum(jnp.where(match, expert_logits, 0.0), axis=-1, keepdims=True) for match in matches
    ]
    highest = functools.reduce(jnp.maximum, picked)
    picked = [jnp.exp(p - highest) for p in picked]
    picked_sum = functools.reduce(jnp.add, picked)
    table = jnp.zeros((rows, experts), F32)
    for visit, match, p in zip(visited, matches, picked):
        chosen = jnp.zeros((rows, 1), F32)
        for g in range(groups):
            inside = (visit >= g * per_group) & (visit < (g + 1) * per_group)
            chosen = chosen + jnp.where(inside, group_prob[:, g : g + 1], 0.0)
        table = table + jnp.where(match, chosen * (p / picked_sum), 0.0)
    padded = jnp.concatenate([table, jnp.zeros((rows, rows - experts), F32)], axis=1)
    tables[0] = padded.T[: tables.shape[1]]
    table_waits = to_all(1, lambda other: tables.at[0], lambda position: tables.at[position])

    take_keys.wait()
    take_values.wait()
    for copy in halo:
        copy.wait_recv()
    local_heads = slopes.shape[0]
    per_kv = HEADS // KV_HEADS

    def attend_block(block, carry):
        start = pl.multiple_of(block * WINDOW, WINDOW)
        q = queries[pl.ds(start, WINDOW)]
        k = key_rows[pl.ds(start, 2 * WINDOW)]
        v = value_rows[pl.ds(start, 2 * WINDOW)]
        query_index = lax.broadcasted_iota(jnp.int32, (WINDOW, 2 * WINDOW), 0)
        key_index = lax.broadcasted_iota(jnp.int32, (WINDOW, 2 * WINDOW), 1)
        distance = query_index + WINDOW - key_index
        position = me_ep * group_rows + start + key_index - WINDOW
        valid = (distance >= 0) & (distance < WINDOW) & (position >= 0)
        far = distance.astype(F32)
        outs = []
        for h in range(local_heads):
            kv = (me_tp * local_heads + h) // per_kv
            own = q[:, h * HD : (h + 1) * HD]
            nothing = jnp.zeros_like(own)
            spread = jnp.concatenate(
                [jnp.where(kv == i, own, nothing) for i in range(KV_HEADS)], axis=1
            )
            scores = lax.dot_general(
                spread, k, (((1,), (1,)), ((), ())), preferred_element_type=F32
            ) * (1.0 / math.sqrt(HD))
            scores = jnp.where(valid, scores - slopes[h] * far, -jnp.inf)
            top = jnp.maximum(jnp.max(scores, axis=-1, keepdims=True), sinks[h])
            weights = jnp.exp(scores - top)
            denom = jnp.sum(weights, axis=-1, keepdims=True) + jnp.exp(sinks[h] - top)
            probs = (weights / denom).astype(BF16)
            mixed = jnp.dot(probs, v, preferred_element_type=F32)
            outs.append(
                sum(
                    jnp.where(kv == i, mixed[:, i * HD : (i + 1) * HD], 0.0)
                    for i in range(KV_HEADS)
                )
            )
        joined = outs[0] if local_heads == 1 else jnp.concatenate(outs, axis=1)
        attended[pl.ds(start, WINDOW)] = joined.astype(BF16)
        return carry

    lax.fori_loop(0, group_rows // WINDOW, attend_block, 0)

    def attended_of(index):
        return pl.ds(pl.multiple_of(index * rows, rows), rows)

    piece_waits = to_all(
        2, lambda other: attended.at[attended_of(other)], lambda position: pieces.at[position]
    )
    pieces[0] = attended[attended_of(me_tp)]

    gate_spread.forward()
    up_spread.forward()
    for spread in down_spreads[:4]:
        for step in range(len(forth)):
            spread.first(step)
    for step in range(1, steps):
        for position in range(1, 1 << step):
            token_wait(position)
            token_send(position, step)
    take_share.wait()
    share_rows = out_weight.shape[0]
    share_waits = {}

    def share_send(position, step):
        target = position + (1 << step)
        share_waits[target] = send(
            share.at[0, pl.ds(position * share_rows, share_rows)],
            share.at[0, pl.ds(target * share_rows, share_rows)],
            tp_send.at[3, target],
            tp_recv.at[3, target],
            {"tp": flipped(me_tp, tp_order[step])},
        )

    share_ready = {0}

    def share_wait(position):
        if position not in share_ready:
            share_waits[position].wait_recv()
            share_ready.add(position)

    for step in range(steps):
        share_send(0, step)

    take_gate.wait()
    take_up.wait()
    for copy in table_waits:
        copy.wait_recv()

    def hidden_part(offset, inner, first, count):
        span = pl.ds(first * rows, count * rows)
        weight = jnp.concatenate([gates[offset, inner], ups[offset, inner]], axis=1)
        both = jnp.dot(tokens[span], weight, preferred_element_type=F32)
        gated, upped = both[:, :units], both[:, units:]
        expert = partner_of(me_ep, offset, n_ep) * local + inner
        amounts = []
        for position in range(first, first + count):
            block = tables[position]
            expert_row = lax.broadcasted_iota(jnp.int32, block.shape, 0)
            line = jnp.sum(jnp.where(expert_row == expert, block, 0.0), axis=0, keepdims=True)
            amounts.append(jnp.broadcast_to(line, (rows, rows)).T)
        amount = jnp.concatenate(amounts, axis=0)[:, :units]
        product = gated / (1.0 + jnp.exp(-gated)) * upped * amount
        product = jnp.where(amount > 0, product, 0.0).astype(BF16)
        place = (offset * local + inner) * units
        hidden[span, place : place + units] = product

    side = n_tp // 2
    early = n_tp // 4 + 1
    ranges = [(0, early), (side, early), (early, side - early), (side + early, side - early)]

    def hidden_parts(offset, wanted):
        gate_spread.wait(offset)
        up_spread.wait(offset)
        for first, count in wanted:
            for position in range(first, first + count):
                token_wait(position)
            for inner in range(local):
                hidden_part(offset, inner, first, count)

    for offset in range(n_ep - 1):
        hidden_parts(offset, ranges[:2])
    for step in range(1, steps):
        for position in range(1, 1 << step):
            share_wait(position)
            share_send(position, step)
    for spread in down_spreads[:2]:
        spread.forward()
    for spread in down_spreads[4:]:
        for step in range(len(forth)):
            spread.first(step)
    for offset in range(n_ep - 1):
        hidden_parts(offset, ranges[2:])
    hidden_parts(n_ep - 1, [(0, side), (side, side)])

    take_down.wait()
    rs_order = tp_order[::-1]
    arrivals = {}
    for copy in sent:
        pass
    token_copies = [coming[position] for position in coming]
    for copy in token_copies:
        copy.wait_send()
    waited = set(id(copy) for copy in token_copies)

    def columns_of(c):
        return pl.ds(c * chunk, chunk)

    def down_of(c):
        return jnp.concatenate(
            [
                downs[offset, inner, c * chunk : (c + 1) * chunk]
                for offset in range(n_ep)
                for inner in range(local)
            ],
            axis=1,
        )

    def down_dot(c, first, count):
        return lax.dot_general(
            hidden[pl.ds(first * rows, count * rows)],
            down_of(c),
            (((1,), (1,)), ((), ())),
            preferred_element_type=F32,
        )

    def reduce_send(c, step):
        count = n_tp >> (step + 1)
        source = tokens.at[pl.ds(count * rows, count * rows), columns_of(c)]
        target = landed.at[pl.ds((count - 1) * rows, count * rows), columns_of(c)]
        arrivals[c, step] = send(
            source,
            target,
            rs_send.at[c, step],
            rs_recv.at[c, step],
            {"tp": flipped(me_tp, rs_order[step])},
        )

    def arrived(c, step):
        count = n_tp >> (step + 1)
        arrivals[c, step].wait_recv()
        return landed[pl.ds((count - 1) * rows, count * rows), columns_of(c)].astype(F32)

    def keep(c, value, count):
        upper = count // 2
        if count > 1:
            tokens[pl.ds(upper * rows, upper * rows), columns_of(c)] = value[upper * rows :].astype(
                BF16
            )
            total[pl.ds(0, upper * rows), columns_of(c)] = value[: upper * rows]
        else:
            total[pl.ds(0, rows), columns_of(c)] = value

    def reduce_open(c):
        for spread in down_spreads[2 * c : 2 * c + 2]:
            for offset in range(1, n_ep):
                spread.wait(offset)
        tokens[pl.ds(side * rows, side * rows), columns_of(c)] = down_dot(c, side, side).astype(BF16)
        reduce_send(c, 0)

    def reduce_second(c):
        value = down_dot(c, 0, side)
        keep(c, value + arrived(c, 0), side)
        reduce_send(c, 1)

    def reduce_step(c, step):
        count = n_tp >> (step + 1)
        keep(c, total[pl.ds(0, count * rows), columns_of(c)] + arrived(c, step), count)
        if step + 1 < steps:
            reduce_send(c, step + 1)

    def project(offset):
        for spread in share_spreads:
            spread.wait(offset)
        joined = jnp.concatenate([pieces[position] for position in range(n_tp)], axis=1)
        place = pl.multiple_of(partner_of(me_ep, offset, n_ep) * columns, columns)
        projected[:, pl.ds(place, columns)] = jnp.dot(
            joined, share[offset], preferred_element_type=F32
        )

    later = [(c, step) for c in range(CHUNKS) for step in range(2, steps)]

    reduce_open(0)
    reduce_second(0)
    for spread in down_spreads[2:4]:
        spread.forward()
    reduce_open(1)
    reduce_second(1)
    for spread in down_spreads[4:6]:
        spread.forward()
    for position in range(1, n_tp):
        share_wait(position)
    for spread in share_spreads:
        for step in range(len(forth)):
            spread.first(step)
    reduce_step(0, 1)
    reduce_open(2)
    reduce_second(2)
    for spread in down_spreads[6:8]:
        spread.forward()
    reduce_step(1, 1)
    reduce_open(3)
    reduce_second(3)
    for spread in share_spreads:
        spread.forward()
    reduce_step(2, 1)
    for step in range(2, steps):
        reduce_step(0, step)
    reduce_step(3, 1)
    for copy in piece_waits:
        copy.wait_recv()
    for offset in range(n_ep):
        project(offset)
    mixer_output[...] = scale_rows(projected[...], mix_gain[...]).astype(BF16)
    for c in range(1, CHUNKS):
        for step in range(2, steps):
            reduce_step(c, step)
    moe_output[...] = scale_rows(total[pl.ds(0, rows)], out_gain[...]).astype(BF16)

    for copy in sent:
        if id(copy) not in waited:
            copy.wait_send()


def per_device(n_ep, n_tp, *arguments):
    (queries, keys, values, slopes, sinks, out_weight, mix_gain, moe_input, in_gain, out_gain) = (
        arguments[:10]
    )
    group_router, expert_router, routes, gate_weight, up_weight, down_weight = arguments[10:]
    rows, width = moe_input.shape
    group_rows = rows * n_tp
    local, _, units = gate_weight.shape
    columns = width // n_ep
    experts = expert_router.shape[1]
    whole = pl.BlockSpec(memory_space=pltpu.VMEM)
    scalar = pl.BlockSpec(memory_space=pltpu.SMEM)
    outside = pl.BlockSpec(memory_space=pl.ANY)
    steps = (n_tp - 1).bit_length()
    copies = 6 + 2 * CHUNKS
    return pl.pallas_call(
        functools.partial(kernel, n_ep, n_tp),
        out_shape=[jax.ShapeDtypeStruct((rows, width), BF16)] * 2,
        in_specs=[
            whole,
            outside,
            outside,
            scalar,
            scalar,
            outside,
            whole,
            whole,
            whole,
            whole,
            whole,
            whole,
            whole,
            outside,
            outside,
            outside,
        ],
        out_specs=[whole, whole],
        scratch_shapes=[
            pltpu.VMEM((n_ep, local, width, units), BF16),
            pltpu.VMEM((n_ep, local, width, units), BF16),
            pltpu.VMEM((n_ep, local, width, units), BF16),
            pltpu.VMEM((group_rows, width), BF16),
            pltpu.VMEM((n_tp, max(8, experts), rows), F32),
            pltpu.VMEM((WINDOW + group_rows, keys.shape[1]), BF16),
            pltpu.VMEM((WINDOW + group_rows, values.shape[1]), BF16),
            pltpu.VMEM(queries.shape, BF16),
            pltpu.VMEM((n_tp, rows, queries.shape[1]), BF16),
            pltpu.VMEM((n_ep, out_weight.shape[0] * n_tp, columns), BF16),
            pltpu.VMEM((rows, width), F32),
            pltpu.VMEM((group_rows, n_ep * local * units), BF16),
            pltpu.VMEM((group_rows - rows, width), BF16),
            pltpu.VMEM((group_rows // 4, width), F32),
            pltpu.SemaphoreType.DMA((8,)),
            pltpu.SemaphoreType.DMA((copies, n_ep)),
            pltpu.SemaphoreType.DMA((copies, n_ep)),
            pltpu.SemaphoreType.DMA((4, n_tp)),
            pltpu.SemaphoreType.DMA((4, n_tp)),
            pltpu.SemaphoreType.DMA((CHUNKS, steps)),
            pltpu.SemaphoreType.DMA((CHUNKS, steps)),
        ],
        compiler_params=pltpu.CompilerParams(
            collective_id=0, has_side_effects=True, vmem_limit_bytes=67000000
        ),
    )(
        queries,
        keys,
        values,
        slopes,
        sinks,
        out_weight,
        mix_gain[None],
        moe_input,
        in_gain[None],
        out_gain[None],
        group_router,
        expert_router,
        routes,
        gate_weight,
        up_weight,
        down_weight,
    )


def solution(mesh):
    return jax.shard_map(
        functools.partial(per_device, mesh.shape["ep"], mesh.shape["tp"]),
        mesh=mesh,
        in_specs=(
            P("ep", "tp"),
            P("ep", None),
            P("ep", None),
            P("tp"),
            P("tp"),
            P("tp", None),
            P(),
            P(("ep", "tp"), None),
            P(),
            P(),
            P(),
            P(),
            P(("ep", "tp"), None),
            P("ep", None, "tp"),
            P("ep", None, "tp"),
            P("ep", None, "tp"),
        ),
        out_specs=(P(("ep", "tp"), None), P(("ep", "tp"), None)),
        check_vma=False,
    )
```

profile of v0, /device:TPU:9, one launch (start us, length us, event | category | flops | bytes accessed | tf_op | source)
XLA Modules:
  0.0 126.8 jit_solution(13970108437010113105)
XLA Ops:
  0.6 0.0 copy-start.3
  0.6 0.7 copy-done.3
  1.3 0.0 copy-start.1
  1.3 0.7 copy.20.routes
  2.0 0.0 copy-done.1
  2.0 0.0 copy-start.2
  2.1 1.1 copy.18.group_router
  3.1 0.0 copy-done.2
  3.1 1.1 copy.19.expert_router
  4.2 119.9 %shard_map.167 = (bf16[128,2048]{1,0:T(8,128)(2,1)}, bf16[128,2048]{1,0:T(8,128)(2,1)}) custom-call(bf16[1024,128]{1,0:T(8,128)(2,1)} %queries.1, bf16[1024,256]{1,0:T(8,128)(2,1)} %keys.1, bf16[1024,256]{1,0:T(8,128)(2,1)} %values.1, f32[2]{0:T(128)} %slopes.1, f32[2]{0:T(128)} %sinks.1, bf16[128,2048]{1,0:T(8,128)(2,1)} %out_weight.1, f32[1,2048]{1,0:T(1,128)} %bitcast.3, ...), custom_call_target="tpu_custom_call" | custom-call | tf_op jit(solution)/shard_map/pallas_call | solution.py:575
  124.1 0.0 copy-start
  124.1 1.9 %copy.23 = bf16[128,2048]{1,0:T(8,128)(2,1)} copy(bf16[128,2048]{1,0:T(8,128)(2,1)} %get-tuple-element.4) | data formatting | bytes 1048576
  126.0 0.0 copy-done
  126.0 0.8 copy.24
Async XLA Ops:
  0.6 0.7 copy-start.3
  1.3 0.7 copy-start.1
  2.0 1.1 copy-start.2
  124.1 2.0 %copy-start = (bf16[128,2048]{1,0:T(8,128)(2,1)S(1)}, bf16[128,2048]{1,0:T(8,128)(2,1)}, u32[]{:S(2)}) copy-start(bf16[128,2048]{1,0:T(8,128)(2,1)} %get-tuple-element.5) | copy-start | bytes 1572868
where the time goes:
time: 127 us
  Pallas kernels  120 us (94%)
  local copies, waits for them, and re-layouts  6.26 us (5%)
    pallas_call x1, Pallas kernels, per_device(): pl.pallas_call(functools.partial(kernel, n_ep, n_tp), out_shape=[jax.Shap...  120 us
    unnamed x13, local copies, waits for them, and re-layouts  6.26 us

commit v1 on v0

v1 whole, which is shorter than its diff:
```python
import functools
import math

import jax
import jax.numpy as jnp
from jax import lax
from jax.experimental import pallas as pl
from jax.experimental.pallas import tpu as pltpu
from jax.sharding import PartitionSpec as P

HEADS = 16
HD = 64
KV_HEADS = 4
WINDOW = 128
CHUNKS = 8
LAG = 2
SHARE_FIRST = 2
SHARE_ON = 6


eps = 1e-06
MESH = pl.DeviceIdType.MESH
F32 = jnp.float32
BF16 = jnp.bfloat16


def flipped(index, bit):
    return index + bit - 2 * bit * ((index // bit) % 2)


def partner_of(index, offset, size):
    bit = 1
    while bit < size:
        if offset & bit:
            index = flipped(index, bit)
        bit *= 2
    return index


def bits_of(size):
    return [1 << i for i in range((size - 1).bit_length())]


def offsets_of(order):
    offsets = [0]
    for bit in order:
        offsets = offsets + [offset ^ bit for offset in offsets]
    return offsets


def scale_rows(matrix, gain):
    mean_square = jnp.mean(matrix * matrix, axis=-1, keepdims=True)
    return matrix * lax.rsqrt(mean_square + eps) * gain


def kernel(
    n_ep,
    n_tp,
    queries_out,
    keys,
    values,
    slopes,
    sinks,
    out_weight,
    moe_input_out,
    in_gain_out,
    group_router_out,
    expert_router_out,
    routes_out,
    gate_weight,
    up_weight,
    down_weight,
    projected,
    total,
    queries,
    in_gain,
    group_router,
    expert_router,
    routes,
    gates,
    ups,
    downs,
    tokens,
    tables,
    key_rows,
    value_rows,
    pieces,
    share,
    hidden,
    landed,
    held,
    local_sem,
    ep_send,
    ep_recv,
    tp_send,
    tp_recv,
    rs_send,
    rs_recv,
):
    me_ep, me_tp = lax.axis_index("ep"), lax.axis_index("tp")
    rows, width = moe_input_out.shape
    local, _, units = gate_weight.shape
    group_rows = rows * n_tp
    columns = width // n_ep
    chunk = width // CHUNKS
    forth = bits_of(n_ep)
    back = forth[::-1]
    tp_order = bits_of(n_tp)[::-1]
    tp_offsets = offsets_of(tp_order)
    cut = share.shape[1] // 4

    sent = []
    locals_ = []

    class Tracked:
        def __init__(self, copy):
            self.copy, self.gone, self.here = copy, False, False

        def start(self):
            self.copy.start()

        def wait_send(self):
            if not self.gone:
                self.copy.wait_send()
                self.gone = True

        def wait_recv(self):
            if not self.here:
                self.copy.wait_recv()
                self.here = True

    def local_copy(source, target):
        copy = pltpu.make_async_copy(source, target, local_sem.at[len(locals_)])
        copy.start()
        locals_.append(copy)
        return copy

    def send(source, target, send_sem, recv_sem, where, started=True):
        copy = pltpu.make_async_remote_copy(
            src_ref=source,
            dst_ref=target,
            send_sem=send_sem,
            recv_sem=recv_sem,
            device_id=where,
            device_id_type=MESH,
        )
        if started:
            copy.start()
        sent.append(Tracked(copy))
        return sent[-1]

    class Spread:
        def __init__(self, number, own, slot_of, order):
            self.number, self.own, self.slot_of, self.order = number, own, slot_of, order
            self.coming = {}

        def post(self, source, offset, bit):
            target = offset ^ bit
            self.coming[target] = send(
                source,
                self.slot_of(target),
                ep_send.at[self.number, target],
                ep_recv.at[self.number, target],
                {"ep": flipped(me_ep, bit)},
            )

        def first(self, step):
            self.post(self.own, 0, self.order[step])

        def wait(self, offset):
            if offset:
                self.coming[offset].wait_recv()

        def forward(self):
            held = [0]
            for bit in self.order:
                for offset in held:
                    if offset:
                        self.wait(offset)
                        self.post(self.slot_of(offset), offset, bit)
                held = held + [offset ^ bit for offset in held]

    gate_spread = Spread(0, gate_weight, lambda o: gates.at[o], forth)
    up_spread = Spread(1, up_weight, lambda o: ups.at[o], back)
    share_spreads = [
        Spread(
            2 + part,
            share.at[0, pl.ds(part * cut, cut)],
            lambda o, part=part: share.at[o, pl.ds(part * cut, cut)],
            order,
        )
        for part, order in ((0, forth), (1, back))
    ]
    halo_number = 4
    down_number = 6

    ep_next = lax.rem(me_ep + 1, n_ep)
    barrier = pltpu.get_barrier_semaphore()
    greeted = [{"ep": partner_of(me_ep, offset, n_ep)} for offset in range(1, n_ep)]
    greeted += [{"tp": flipped(me_tp, bit)} for bit in tp_order]
    for where in greeted:
        pl.semaphore_signal(barrier, inc=1, device_id=where, device_id_type=MESH)
    take_input = [
        local_copy(moe_input_out, tokens.at[pl.ds(0, moe_input_out.shape[0])]),
        local_copy(in_gain_out, in_gain),
    ]
    take_router = [
        local_copy(group_router_out, group_router),
        local_copy(expert_router_out, expert_router),
        local_copy(routes_out, routes),
    ]
    take_rows = [
        local_copy(keys, key_rows.at[pl.ds(WINDOW, group_rows)]),
        local_copy(values, value_rows.at[pl.ds(WINDOW, group_rows)]),
        local_copy(queries_out, queries),
    ]
    take_gate = local_copy(gate_weight, gates.at[0])
    take_up = local_copy(up_weight, ups.at[0])
    take_down = local_copy(down_weight, downs.at[0])
    own_columns = pl.ds(pl.multiple_of(me_ep * columns, columns), columns)
    take_share = local_copy(out_weight.at[:, own_columns], share.at[0, pl.ds(0, out_weight.shape[0])])
    pl.semaphore_wait(barrier, len(greeted))

    core = lax.rem(me_tp, 2)

    def start_by_core(copies):
        @pl.when(core == 0)
        def _():
            for copy in copies:
                copy.start()

        @pl.when(core == 1)
        def _():
            for copy in copies[::-1]:
                copy.start()

    for step in range(len(forth)):
        gate_spread.first(step)
        up_spread.first(step)
        if step == 0:
            halo = []
            last_rows = pl.ds(group_rows - WINDOW, WINDOW)
            for place, (source, target) in enumerate(((keys, key_rows), (values, value_rows))):
                halo.append(
                    send(
                        source.at[last_rows],
                        target.at[pl.ds(0, WINDOW)],
                        ep_send.at[halo_number + place, 0],
                        ep_recv.at[halo_number + place, 0],
                        {"ep": ep_next},
                    )
                )

    for copy in take_input:
        copy.wait()
    normed = scale_rows(tokens[pl.ds(0, rows)].astype(F32), in_gain[...]).astype(BF16)
    tokens[pl.ds(0, rows)] = normed
    for copy in take_router:
        copy.wait()

    def logits_of(router):
        return lax.dot_general(
            router[...], normed, (((1,), (1,)), ((), ())), preferred_element_type=F32
        )

    group_logits, expert_logits = logits_of(group_router), logits_of(expert_router)
    experts, groups = expert_logits.shape[0], group_logits.shape[0]
    per_group = experts // groups
    group_shifted = jnp.exp(group_logits - jnp.max(group_logits, axis=0, keepdims=True))
    group_prob = group_shifted / jnp.sum(group_shifted, axis=0, keepdims=True)
    expert_ids = lax.broadcasted_iota(jnp.int32, (experts, rows), 0)
    visited = [routes[k : k + 1] for k in range(routes.shape[0])]
    matches = [expert_ids == visit for visit in visited]
    picked = [
        jnp.sum(jnp.where(match, expert_logits, 0.0), axis=0, keepdims=True) for match in matches
    ]
    highest = functools.reduce(jnp.maximum, picked)
    picked = [jnp.exp(p - highest) for p in picked]
    picked_sum = functools.reduce(jnp.add, picked)
    table = jnp.zeros((experts, rows), F32)
    for visit, match, p in zip(visited, matches, picked):
        chosen = jnp.zeros((1, rows), F32)
        for g in range(groups):
            inside = (visit >= g * per_group) & (visit < (g + 1) * per_group)
            chosen = chosen + jnp.where(inside, group_prob[g : g + 1], 0.0)
        table = table + jnp.where(match, chosen * (p / picked_sum), 0.0)
    tables[0] = jnp.zeros(tables.shape[1:], F32)
    tables[0, pl.ds(0, experts)] = table

    coming = {}
    steps = len(tp_order)

    def span_of(position):
        return pl.ds(position * rows, rows)

    def token_send(position, step, started=True):
        target = position + (1 << step)
        where = {"tp": flipped(me_tp, tp_order[step])}
        coming[target] = [
            send(
                source.at[at],
                source.at[to],
                tp_send.at[number, target],
                tp_recv.at[number, target],
                where,
                started,
            )
            for number, source, at, to in (
                (1, tables, position, target),
                (0, tokens, span_of(position), span_of(target)),
            )
        ]
        return coming[target]

    def token_wait(position):
        if position:
            for copy in coming[position]:
                copy.wait_recv()

    token_send(0, steps - 1)
    start_by_core([copy for step in range(steps - 1) for copy in token_send(0, step, False)])

    def to_all(number, source_of, target_of):
        waits = []
        for position in range(1, n_tp):
            other = partner_of(me_tp, tp_offsets[position], n_tp)
            waits.append(
                send(
                    source_of(other),
                    target_of(position),
                    tp_send.at[number, position],
                    tp_recv.at[number, position],
                    {"tp": other},
                )
            )
        return waits

    for copy in take_rows:
        copy.wait()
    for copy in halo:
        copy.wait_recv()
    local_heads = slopes.shape[0]
    per_kv = HEADS // KV_HEADS

    def attend_block(block, carry):
        start = pl.multiple_of(block * WINDOW, WINDOW)
        q = queries[pl.ds(start, WINDOW)]
        k = key_rows[pl.ds(start, 2 * WINDOW)]
        v = value_rows[pl.ds(start, 2 * WINDOW)]
        query_index = lax.broadcasted_iota(jnp.int32, (WINDOW, 2 * WINDOW), 0)
        key_index = lax.broadcasted_iota(jnp.int32, (WINDOW, 2 * WINDOW), 1)
        distance = query_index + WINDOW - key_index
        position = me_ep * group_rows + start + key_index - WINDOW
        valid = (distance >= 0) & (distance < WINDOW) & (position >= 0)
        far = distance.astype(F32)
        outs = []
        for h in range(local_heads):
            kv = (me_tp * local_heads + h) // per_kv
            own = q[:, h * HD : (h + 1) * HD]
            nothing = jnp.zeros_like(own)
            spread = jnp.concatenate(
                [jnp.where(kv == i, own, nothing) for i in range(KV_HEADS)], axis=1
            )
            scores = lax.dot_general(
                spread, k, (((1,), (1,)), ((), ())), preferred_element_type=F32
            ) * (1.0 / math.sqrt(HD))
            scores = jnp.where(valid, scores - slopes[h] * far, -jnp.inf)
            top = jnp.maximum(jnp.max(scores, axis=-1, keepdims=True), sinks[h])
            weights = jnp.exp(scores - top)
            denom = jnp.sum(weights, axis=-1, keepdims=True) + jnp.exp(sinks[h] - top)
            probs = (weights / denom).astype(BF16)
            mixed = jnp.dot(probs, v, preferred_element_type=F32)
            outs.append(
                sum(
                    jnp.where(kv == i, mixed[:, i * HD : (i + 1) * HD], 0.0)
                    for i in range(KV_HEADS)
                )
            )
        joined = outs[0] if local_heads == 1 else jnp.concatenate(outs, axis=1)
        queries[pl.ds(start, WINDOW)] = joined.astype(BF16)
        return carry

    lax.fori_loop(0, group_rows // WINDOW, attend_block, 0)

    def attended_of(index):
        return pl.ds(pl.multiple_of(index * rows, rows), rows)

    pieces[0] = queries[attended_of(me_tp)]

    gate_spread.forward()
    up_spread.forward()

    down_waits = {}
    for c in range(CHUNKS):
        span = pl.ds(c * chunk, chunk)
        for offset in range(1, n_ep):
            down_waits[c, offset] = send(
                down_weight.at[:, span],
                downs.at[offset, :, span],
                ep_send.at[down_number + c, offset],
                ep_recv.at[down_number + c, offset],
                {"ep": partner_of(me_ep, offset, n_ep)},
            )
    for step in range(1, steps):
        for position in range(1, 1 << step):
            token_wait(position)
            token_send(position, step)

    take_gate.wait()
    take_up.wait()

    def hidden_part(offset, inner, first, count):
        span = pl.ds(first * rows, count * rows)
        weight = jnp.concatenate([gates[offset, inner], ups[offset, inner]], axis=1)
        both = jnp.dot(tokens[span], weight, preferred_element_type=F32)
        gated, upped = both[:, :units], both[:, units:]
        expert = partner_of(me_ep, offset, n_ep) * local + inner
        amounts = []
        for position in range(first, first + count):
            block = tables[position]
            expert_row = lax.broadcasted_iota(jnp.int32, block.shape, 0)
            line = jnp.sum(jnp.where(expert_row == expert, block, 0.0), axis=0, keepdims=True)
            amounts.append(jnp.broadcast_to(line, (rows, rows)).T)
        amount = jnp.concatenate(amounts, axis=0)[:, :units]
        product = gated / (1.0 + jnp.exp(-gated)) * upped * amount
        product = jnp.where(amount > 0, product, 0.0).astype(BF16)
        place = (offset * local + inner) * units
        hidden[span, place : place + units] = product

    side = n_tp // 2
    early = n_tp // 4 + 1
    ranges = [(0, early), (side, early), (early, side - early), (side + early, side - early)]

    def hidden_parts(offset, wanted):
        gate_spread.wait(offset)
        up_spread.wait(offset)
        for first, count in wanted:
            for position in range(first, first + count):
                token_wait(position)
            for inner in range(local):
                hidden_part(offset, inner, first, count)

    for offset in range(n_ep - 1):
        hidden_parts(offset, ranges[:2])
    for offset in range(n_ep - 1):
        hidden_parts(offset, ranges[2:])
    piece_waits = to_all(
        2, lambda other: queries.at[attended_of(other)], lambda position: pieces.at[position]
    )
    take_share.wait()
    share_rows = out_weight.shape[0]
    share_waits = {}

    def share_send(position, step, started=True):
        target = position + (1 << step)
        share_waits[target] = send(
            share.at[0, pl.ds(position * share_rows, share_rows)],
            share.at[0, pl.ds(target * share_rows, share_rows)],
            tp_send.at[3, target],
            tp_recv.at[3, target],
            {"tp": flipped(me_tp, tp_order[step])},
            started,
        )
        return share_waits[target]

    def share_wait(position):
        if position:
            share_waits[position].wait_recv()

    start_by_core([share_send(0, step, False) for step in range(steps - 1)])
    hidden_parts(n_ep - 1, [(0, side), (side, side)])

    take_down.wait()
    rs_order = tp_order[::-1]
    arrivals = {}
    for position in coming:
        for copy in coming[position]:
            copy.wait_send()

    def columns_of(c):
        return pl.ds(c * chunk, chunk)

    def down_of(c):
        return jnp.concatenate(
            [
                downs[offset, inner, c * chunk : (c + 1) * chunk]
                for offset in range(n_ep)
                for inner in range(local)
            ],
            axis=1,
        )

    def down_dot(c, first, count):
        return lax.dot_general(
            hidden[pl.ds(first * rows, count * rows)],
            down_of(c),
            (((1,), (1,)), ((), ())),
            preferred_element_type=F32,
        )

    def reduce_send(c, step, started=True):
        count = n_tp >> (step + 1)
        arrivals[c, step] = send(
            tokens.at[pl.ds(count * rows, count * rows), columns_of(c)],
            landed.at[pl.ds((count - 1) * rows, count * rows), columns_of(c)],
            rs_send.at[c, step],
            rs_recv.at[c, step],
            {"tp": flipped(me_tp, rs_order[step])},
            started,
        )
        return arrivals[c, step]

    def arrived(c, step):
        count = n_tp >> (step + 1)
        arrivals[c, step].wait_recv()
        return landed[pl.ds((count - 1) * rows, count * rows), columns_of(c)].astype(F32)

    def keep(c, value, count):
        upper = count // 2
        tokens[pl.ds(upper * rows, upper * rows), columns_of(c)] = value[upper * rows :].astype(BF16)
        held[pl.ds(0, upper * rows), columns_of(c)] = value[: upper * rows]

    def reduce_open(c):
        for offset in range(1, n_ep):
            down_waits[c, offset].wait_recv()
        tokens[pl.ds(side * rows, side * rows), columns_of(c)] = down_dot(c, side, side).astype(BF16)
        reduce_send(c, 0)
        return down_dot(c, 0, side)

    def reduce_kept(c, step):
        count = n_tp >> (step + 1)
        return held[pl.ds(0, count * rows), columns_of(c)] + arrived(c, step)

    crossed = {}

    def share_across(offset):
        for spread in share_spreads:
            spread.wait(offset)
        crossed[offset] = send(
            share.at[offset, pl.ds(0, 2 * cut)],
            share.at[offset, pl.ds(2 * cut, 2 * cut)],
            tp_send.at[4, offset],
            tp_recv.at[4, offset],
            {"tp": flipped(me_tp, 1)},
        )

    def project(offset):
        if offset not in crossed:
            share_across(offset)
        crossed[offset].wait_recv()
        joined = jnp.concatenate([pieces[position] for position in range(n_tp)], axis=1)
        place = pl.multiple_of(partner_of(me_ep, offset, n_ep) * columns, columns)
        projected[:, pl.ds(place, columns)] = jnp.dot(
            joined, share[offset], preferred_element_type=F32
        )

    for tick in range(CHUNKS + LAG * (steps - 1)):
        leaving = []
        if tick < CHUNKS:
            value = reduce_open(tick)
            keep(tick, value + arrived(tick, 0), side)
            leaving.append(reduce_send(tick, 1, False))
        for step in range(1, steps - 1):
            c = tick - LAG * step
            if 0 <= c < CHUNKS:
                keep(c, reduce_kept(c, step), n_tp >> (step + 1))
                leaving.append(reduce_send(c, step + 1, False))
        if leaving:
            start_by_core(leaving)
        c = tick - LAG * (steps - 1)
        if c >= 0:
            total[:, columns_of(c)] = reduce_kept(c, steps - 1)
        if tick == 0:
            for step in range(1, steps - 1):
                for position in range(1, 1 << step):
                    share_wait(position)
                    share_send(position, step)
        if tick == SHARE_FIRST:
            for position in range(1, side):
                share_wait(position)
            share_across(0)
            for step in range(len(forth)):
                for spread in share_spreads:
                    spread.first(step)
        if tick == SHARE_ON:
            for spread in share_spreads:
                spread.forward()
            for offset in forth:
                share_across(offset)
            for copy in piece_waits:
                copy.wait_recv()
            project(0)

    for offset in range(1, n_ep):
        if offset not in crossed:
            share_across(offset)
    for offset in range(1, n_ep):
        project(offset)
    for copy in sent:
        copy.wait_send()


def finish(projected, total, mix_gain, out_gain, mixer_output, moe_output):
    mixer_output[...] = scale_rows(projected[...], mix_gain[...]).astype(BF16)
    moe_output[...] = scale_rows(total[...], out_gain[...]).astype(BF16)


def per_device(n_ep, n_tp, *arguments):
    (queries, keys, values, slopes, sinks, out_weight, mix_gain, moe_input, in_gain, out_gain) = (
        arguments[:10]
    )
    group_router, expert_router, routes, gate_weight, up_weight, down_weight = arguments[10:]
    rows, width = moe_input.shape
    group_rows = rows * n_tp
    local, _, units = gate_weight.shape
    columns = width // n_ep
    experts, groups = expert_router.shape[1], group_router.shape[1]
    whole = pl.BlockSpec(memory_space=pltpu.VMEM)
    scalar = pl.BlockSpec(memory_space=pltpu.SMEM)
    outside = pl.BlockSpec(memory_space=pl.ANY)
    steps = (n_tp - 1).bit_length()
    copies = 6 + CHUNKS
    projected, total = pl.pallas_call(
        functools.partial(kernel, n_ep, n_tp),
        out_shape=[jax.ShapeDtypeStruct((rows, width), F32)] * 2,
        in_specs=[outside] * 3 + [scalar] * 2 + [outside] * 9,
        out_specs=[whole, whole],
        scratch_shapes=[
            pltpu.VMEM(queries.shape, BF16),
            pltpu.VMEM((1, width), F32),
            pltpu.VMEM((groups, width), BF16),
            pltpu.VMEM((experts, width), BF16),
            pltpu.VMEM((routes.shape[1], rows), jnp.int32),
            pltpu.VMEM((n_ep, local, width, units), BF16),
            pltpu.VMEM((n_ep, local, width, units), BF16),
            pltpu.VMEM((n_ep, local, width, units), BF16),
            pltpu.VMEM((group_rows, width), BF16),
            pltpu.VMEM((n_tp, max(8, experts), rows), F32),
            pltpu.VMEM((WINDOW + group_rows, keys.shape[1]), BF16),
            pltpu.VMEM((WINDOW + group_rows, values.shape[1]), BF16),
            pltpu.VMEM((n_tp, rows, queries.shape[1]), BF16),
            pltpu.VMEM((n_ep, out_weight.shape[0] * n_tp, columns), BF16),
            pltpu.VMEM((group_rows, n_ep * local * units), BF16),
            pltpu.VMEM((group_rows - rows, width), BF16),
            pltpu.VMEM((group_rows // 4, width), F32),
            pltpu.SemaphoreType.DMA((16,)),
            pltpu.SemaphoreType.DMA((copies, n_ep)),
            pltpu.SemaphoreType.DMA((copies, n_ep)),
            pltpu.SemaphoreType.DMA((5, max(n_tp, n_ep))),
            pltpu.SemaphoreType.DMA((5, max(n_tp, n_ep))),
            pltpu.SemaphoreType.DMA((CHUNKS, steps)),
            pltpu.SemaphoreType.DMA((CHUNKS, steps)),
        ],
        compiler_params=pltpu.CompilerParams(
            collective_id=0, has_side_effects=True, vmem_limit_bytes=67000000
        ),
    )(
        queries,
        keys,
        values,
        slopes,
        sinks,
        out_weight,
        moe_input,
        in_gain[None],
        group_router.T,
        expert_router.T,
        routes.T,
        gate_weight,
        up_weight,
        down_weight,
    )
    return pl.pallas_call(
        finish,
        out_shape=[jax.ShapeDtypeStruct((rows, width), BF16)] * 2,
        in_specs=[whole] * 4,
        out_specs=[whole] * 2,
    )(projected, total, mix_gain[None], out_gain[None])


def solution(mesh):
    return jax.shard_map(
        functools.partial(per_device, mesh.shape["ep"], mesh.shape["tp"]),
        mesh=mesh,
        in_specs=(
            P("ep", "tp"),
            P("ep", None),
            P("ep", None),
            P("tp"),
            P("tp"),
            P("tp", None),
            P(),
            P(("ep", "tp"), None),
            P(),
            P(),
            P(),
            P(),
            P(("ep", "tp"), None),
            P("ep", None, "tp"),
            P("ep", None, "tp"),
            P("ep", None, "tp"),
        ),
        out_specs=(P(("ep", "tp"), None), P(("ep", "tp"), None)),
        check_vma=False,
    )
```

time: 127 us -> 107 us (0.84)
  the two profiles are of different devices: /device:TPU:9 before, /device:TPU:1 now
where the time goes in v1:
time: 107 us
  Pallas kernels  106 us (99%)
    pallas_call x1, Pallas kernels, per_device(): pl.pallas_call(functools.partial(kernel, n_ep, n_tp), out_shape=[jax.Shap...  103 us
    pallas_call x1, Pallas kernels, per_device(): pl.pallas_call(finish, out_shape=[jax.ShapeDtypeStruct((rows, width), BF1...  2.75 us

profile of v1, /device:TPU:1, one launch (start us, length us, event | category | flops | bytes accessed | tf_op | source)
XLA Modules:
  0.0 106.7 jit_solution(14532377703129493621)
XLA Ops:
  0.6 103.3 %shard_map.167 = (f32[128,2048]{1,0:T(8,128)}, f32[128,2048]{1,0:T(8,128)}) custom-call(bf16[1024,128]{1,0:T(8,128)(2,1)} %queries_out.1, bf16[1024,256]{1,0:T(8,128)(2,1)} %keys.1, bf16[1024,256]{1,0:T(8,128)(2,1)} %values.1, f32[2]{0:T(128)} %slopes.1, f32[2]{0:T(128)} %sinks.1, bf16[128,2048]{1,0:T(8,128)(2,1)} %out_weight.1, ...), custom_call_target="tpu_custom_call" | custom-call | tf_op jit(solution)/shard_map/pallas_call | solution.py:623
  103.9 2.7 %shard_map.168 = (bf16[128,2048]{1,0:T(8,128)(2,1)}, bf16[128,2048]{1,0:T(8,128)(2,1)}) custom-call(f32[128,2048]{1,0:T(8,128)} %get-tuple-element.4.projected, f32[128,2048]{1,0:T(8,128)} %get-tuple-element.5.total, f32[1,2048]{1,0:T(1,128)} %bitcast.9, f32[1,2048]{1,0:T(1,128)} %bitcast.10), custom_call_target="tpu_custom_call" | custom-call | tf_op jit(solution)/shard_map/pallas_call | solution.py:673

commit v2 on v1

--- a/solution.py
+++ b/solution.py
@@ -14,8 +14,6 @@
 WINDOW = 128
 CHUNKS = 8
 LAG = 2
-SHARE_FIRST = 2
-SHARE_ON = 6
 
 
 eps = 1e-06
@@ -39,13 +37,6 @@
 
 def bits_of(size):
     return [1 << i for i in range((size - 1).bit_length())]
-
-
-def offsets_of(order):
-    offsets = [0]
-    for bit in order:
-        offsets = offsets + [offset ^ bit for offset in offsets]
-    return offsets
 
 
 def scale_rows(matrix, gain):
@@ -64,16 +55,18 @@
     out_weight,
     moe_input_out,
     in_gain_out,
+    mix_gain_out,
     group_router_out,
     expert_router_out,
     routes_out,
     gate_weight,
     up_weight,
     down_weight,
-    projected,
+    mixed,
     total,
     queries,
     in_gain,
+    mix_gain,
     group_router,
     expert_router,
     routes,
@@ -86,14 +79,19 @@
     value_rows,
     pieces,
     share,
+    projected,
     hidden,
     landed,
-    held,
+    passing,
     local_sem,
     ep_send,
     ep_recv,
     tp_send,
     tp_recv,
+    core_send,
+    core_recv,
+    all_send,
+    all_recv,
     rs_send,
     rs_recv,
 ):
@@ -103,10 +101,16 @@
     group_rows = rows * n_tp
     columns = width // n_ep
     chunk = width // CHUNKS
+    own_span = pl.ds(pl.multiple_of(lax.axis_index("tp") // 2 * rows, rows), rows)
     forth = bits_of(n_ep)
     back = forth[::-1]
-    tp_order = bits_of(n_tp)[::-1]
-    tp_offsets = offsets_of(tp_order)
+    chips = n_tp // 2
+    chip, core = me_tp // 2, lax.rem(me_tp, 2)
+    sibling = {"tp": flipped(me_tp, 1)}
+    flows = (
+        (1, {"tp": me_tp + 2}, chips - 1 - chip, chip),
+        (-1, {"tp": me_tp - 2}, chip, chips - 1 - chip),
+    )
     cut = share.shape[1] // 4
 
     sent = []
@@ -197,11 +201,17 @@
     ep_next = lax.rem(me_ep + 1, n_ep)
     barrier = pltpu.get_barrier_semaphore()
     greeted = [{"ep": partner_of(me_ep, offset, n_ep)} for offset in range(1, n_ep)]
-    greeted += [{"tp": flipped(me_tp, bit)} for bit in tp_order]
+    greeted += [sibling]
     for where in greeted:
         pl.semaphore_signal(barrier, inc=1, device_id=where, device_id_type=MESH)
+    for _, following, ahead, _ in flows:
+
+        @pl.when(ahead > 0)
+        def _(following=following):
+            pl.semaphore_signal(barrier, inc=1, device_id=following, device_id_type=MESH)
+
     take_input = [
-        local_copy(moe_input_out, tokens.at[pl.ds(0, moe_input_out.shape[0])]),
+        local_copy(moe_input_out, tokens.at[own_span]),
         local_copy(in_gain_out, in_gain),
     ]
     take_router = [
@@ -214,47 +224,44 @@
         local_copy(values, value_rows.at[pl.ds(WINDOW, group_rows)]),
         local_copy(queries_out, queries),
     ]
+    take_mix = local_copy(mix_gain_out, mix_gain)
     take_gate = local_copy(gate_weight, gates.at[0])
     take_up = local_copy(up_weight, ups.at[0])
     take_down = local_copy(down_weight, downs.at[0])
     own_columns = pl.ds(pl.multiple_of(me_ep * columns, columns), columns)
-    take_share = local_copy(out_weight.at[:, own_columns], share.at[0, pl.ds(0, out_weight.shape[0])])
-    pl.semaphore_wait(barrier, len(greeted))
-
-    core = lax.rem(me_tp, 2)
-
-    def start_by_core(copies):
-        @pl.when(core == 0)
-        def _():
-            for copy in copies:
-                copy.start()
-
-        @pl.when(core == 1)
-        def _():
-            for copy in copies[::-1]:
-                copy.start()
-
+    take_share = local_copy(
+        out_weight.at[:, own_columns],
+        share.at[
+            0,
+            pl.ds(
+                pl.multiple_of(me_tp // 2 * out_weight.shape[0], out_weight.shape[0]),
+                out_weight.shape[0],
+            ),
+        ],
+    )
+    neighbours = sum(jnp.where(ahead > 0, 1, 0) for _, _, ahead, _ in flows)
+    pl.semaphore_wait(barrier, len(greeted) + neighbours)
+
+    halo = []
+    last_rows = pl.ds(group_rows - WINDOW, WINDOW)
+    for place, (source, target) in enumerate(((keys, key_rows), (values, value_rows))):
+        halo.append(
+            send(
+                source.at[last_rows],
+                target.at[pl.ds(0, WINDOW)],
+                ep_send.at[halo_number + place, 0],
+                ep_recv.at[halo_number + place, 0],
+                {"ep": ep_next},
+            )
+        )
     for step in range(len(forth)):
         gate_spread.first(step)
         up_spread.first(step)
-        if step == 0:
-            halo = []
-            last_rows = pl.ds(group_rows - WINDOW, WINDOW)
-            for place, (source, target) in enumerate(((keys, key_rows), (values, value_rows))):
-                halo.append(
-                    send(
-                        source.at[last_rows],
-                        target.at[pl.ds(0, WINDOW)],
-                        ep_send.at[halo_number + place, 0],
-                        ep_recv.at[halo_number + place, 0],
-                        {"ep": ep_next},
-                    )
-                )
 
     for copy in take_input:
         copy.wait()
-    normed = scale_rows(tokens[pl.ds(0, rows)].astype(F32), in_gain[...]).astype(BF16)
-    tokens[pl.ds(0, rows)] = normed
+    normed = scale_rows(tokens[own_span].astype(F32), in_gain[...]).astype(BF16)
+    tokens[own_span] = normed
     for copy in take_router:
         copy.wait()
 
@@ -284,56 +291,116 @@
             inside = (visit >= g * per_group) & (visit < (g + 1) * per_group)
             chosen = chosen + jnp.where(inside, group_prob[g : g + 1], 0.0)
         table = table + jnp.where(match, chosen * (p / picked_sum), 0.0)
-    tables[0] = jnp.zeros(tables.shape[1:], F32)
-    tables[0, pl.ds(0, experts)] = table
-
-    coming = {}
-    steps = len(tp_order)
-
-    def span_of(position):
-        return pl.ds(position * rows, rows)
-
-    def token_send(position, step, started=True):
-        target = position + (1 << step)
-        where = {"tp": flipped(me_tp, tp_order[step])}
-        coming[target] = [
-            send(
-                source.at[at],
-                source.at[to],
-                tp_send.at[number, target],
-                tp_recv.at[number, target],
-                where,
-                started,
+    height = tables.shape[0] // n_tp
+    if height > experts:
+        table = jnp.concatenate([table, jnp.zeros((height - experts, rows), F32)], axis=0)
+    tables[pl.ds(pl.multiple_of(chip * height, height), height)] = table
+
+    def span_of(block):
+        return pl.ds(pl.multiple_of(block * rows, rows), rows)
+
+    class Line:
+        def __init__(self, number, ref, part=0, parts=1):
+            self.number, self.ref = number, ref
+            self.height = ref.shape[0] // n_tp // parts
+            self.part, self.parts = part, parts
+
+        def at(self, block):
+            start = (block * self.parts + self.part) * self.height
+            return self.ref.at[pl.ds(pl.multiple_of(start, self.height), self.height)]
+
+        def copy(self, flow, far, block, where):
+            number = 2 * self.number + flow
+            return pltpu.make_async_remote_copy(
+                src_ref=self.at(block),
+                dst_ref=self.at(block),
+                send_sem=tp_send.at[number, far],
+                recv_sem=tp_recv.at[number, far],
+                device_id=where,
+                device_id_type=MESH,
             )
-            for number, source, at, to in (
-                (1, tables, position, target),
-                (0, tokens, span_of(position), span_of(target)),
+
+        def push(self, far, act="start"):
+            for flow, (way, following, ahead, behind) in enumerate(flows):
+
+                @pl.when((ahead > 0) & (behind >= far - 1))
+                def _(flow=flow, way=way, following=following):
+                    getattr(self.copy(flow, far, chip - way * (far - 1), following), act)()
+
+        def take(self, far):
+            for flow, (way, following, ahead, behind) in enumerate(flows):
+
+                @pl.when(behind >= far)
+                def _(flow=flow, way=way):
+                    self.copy(flow, far, chip - way * far, sibling).wait_recv()
+
+    class Across:
+        def __init__(self, line):
+            self.line = line
+
+        def copy(self, flow, far, block):
+            number = 2 * self.line.number + flow
+            return pltpu.make_async_remote_copy(
+                src_ref=self.line.at(block),
+                dst_ref=self.line.at(chips + block),
+                send_sem=core_send.at[number, far],
+                recv_sem=core_recv.at[number, far],
+                device_id=sibling,
+                device_id_type=MESH,
             )
-        ]
-        return coming[target]
-
-    def token_wait(position):
-        if position:
-            for copy in coming[position]:
-                copy.wait_recv()
-
-    token_send(0, steps - 1)
-    start_by_core([copy for step in range(steps - 1) for copy in token_send(0, step, False)])
+
+        def act(self, far, what):
+            if far == 0:
+                getattr(self.copy(0, 0, chip), what)()
+                return
+            for flow, (way, _, _, behind) in enumerate(flows):
+
+                @pl.when(behind >= far)
+                def _(flow=flow, way=way):
+                    getattr(self.copy(flow, far, chip - way * far), what)()
+
+    token_lines = [Line(0, tables), Line(1, tokens, 0, 2), Line(2, tokens, 1, 2)]
+    token_across = [Across(line) for line in token_lines]
+
+    def tokens_on(far):
+        for line in token_lines:
+            if far:
+                line.take(far)
+            if far + 1 < chips:
+                line.push(far + 1)
+        for line in token_across:
+            line.act(far, "start")
+
+    def tokens_across(far):
+        for line in token_across:
+            line.act(far, "wait_recv")
+
+    tokens_on(0)
 
     def to_all(number, source_of, target_of):
         waits = []
-        for position in range(1, n_tp):
-            other = partner_of(me_tp, tp_offsets[position], n_tp)
+        for offset in range(1, n_tp):
+            other = partner_of(me_tp, offset, n_tp)
             waits.append(
                 send(
                     source_of(other),
-                    target_of(position),
-                    tp_send.at[number, position],
-                    tp_recv.at[number, position],
+                    target_of(offset % 2 * chips + chip),
+                    all_send.at[number, offset],
+                    all_recv.at[number, offset],
                     {"tp": other},
+                    False,
                 )
             )
         return waits
+
+    def start_pieces(inner):
+        for offset, copy in zip(range(1, n_tp), piece_waits):
+            place = partner_of(me_tp, offset, n_tp) // 2
+            inside = (place > 0) & (place < chips - 1)
+
+            @pl.when(inside if inner else jnp.logical_not(inside))
+            def _(copy=copy):
+                copy.start()
 
     for copy in take_rows:
         copy.wait()
@@ -385,7 +452,7 @@
     def attended_of(index):
         return pl.ds(pl.multiple_of(index * rows, rows), rows)
 
-    pieces[0] = queries[attended_of(me_tp)]
+    pieces[chip] = queries[attended_of(me_tp)]
 
     gate_spread.forward()
     up_spread.forward()
@@ -401,23 +468,25 @@
                 ep_recv.at[down_number + c, offset],
                 {"ep": partner_of(me_ep, offset, n_ep)},
             )
-    for step in range(1, steps):
-        for position in range(1, 1 << step):
-            token_wait(position)
-            token_send(position, step)
+    for far in range(1, chips - 1):
+        tokens_on(far)
+    take_share.wait()
+    share_line = Line(3, share.at[0])
+    share_line.push(1)
 
     take_gate.wait()
     take_up.wait()
 
     def hidden_part(offset, inner, first, count):
-        span = pl.ds(first * rows, count * rows)
+        span = pl.ds(pl.multiple_of(first * rows, rows), count * rows)
         weight = jnp.concatenate([gates[offset, inner], ups[offset, inner]], axis=1)
         both = jnp.dot(tokens[span], weight, preferred_element_type=F32)
         gated, upped = both[:, :units], both[:, units:]
         expert = partner_of(me_ep, offset, n_ep) * local + inner
         amounts = []
-        for position in range(first, first + count):
-            block = tables[position]
+        height = tables.shape[0] // n_tp
+        for number in range(count):
+            block = tables[pl.ds(pl.multiple_of((first + number) * height, height), height)]
             expert_row = lax.broadcasted_iota(jnp.int32, block.shape, 0)
             line = jnp.sum(jnp.where(expert_row == expert, block, 0.0), axis=0, keepdims=True)
             amounts.append(jnp.broadcast_to(line, (rows, rows)).T)
@@ -427,58 +496,48 @@
         place = (offset * local + inner) * units
         hidden[span, place : place + units] = product
 
-    side = n_tp // 2
-    early = n_tp // 4 + 1
-    ranges = [(0, early), (side, early), (early, side - early), (side + early, side - early)]
-
-    def hidden_parts(offset, wanted):
+    def sweep(wanted, offsets):
+        def block_step(block, carry):
+            far = jnp.abs(lax.rem(block, chips) - chip)
+
+            @pl.when(wanted(far))
+            def _():
+                for offset in offsets:
+                    for inner in range(local):
+                        hidden_part(offset, inner, block, 1)
+
+            return carry
+
+        lax.fori_loop(0, n_tp, block_step, 0)
+
+    for offset in range(n_ep - 1):
         gate_spread.wait(offset)
         up_spread.wait(offset)
-        for first, count in wanted:
-            for position in range(first, first + count):
-                token_wait(position)
-            for inner in range(local):
-                hidden_part(offset, inner, first, count)
-
-    for offset in range(n_ep - 1):
-        hidden_parts(offset, ranges[:2])
-    for offset in range(n_ep - 1):
-        hidden_parts(offset, ranges[2:])
+    for far in range(chips - 1):
+        tokens_across(far)
     piece_waits = to_all(
-        2, lambda other: queries.at[attended_of(other)], lambda position: pieces.at[position]
+        0, lambda other: queries.at[attended_of(other)], lambda place: pieces.at[place]
     )
-    take_share.wait()
-    share_rows = out_weight.shape[0]
-    share_waits = {}
-
-    def share_send(position, step, started=True):
-        target = position + (1 << step)
-        share_waits[target] = send(
-            share.at[0, pl.ds(position * share_rows, share_rows)],
-            share.at[0, pl.ds(target * share_rows, share_rows)],
-            tp_send.at[3, target],
-            tp_recv.at[3, target],
-            {"tp": flipped(me_tp, tp_order[step])},
-            started,
-        )
-        return share_waits[target]
-
-    def share_wait(position):
-        if position:
-            share_waits[position].wait_recv()
-
-    start_by_core([share_send(0, step, False) for step in range(steps - 1)])
-    hidden_parts(n_ep - 1, [(0, side), (side, side)])
+    start_pieces(True)
+    sweep(lambda far: far < chips - 1, range(n_ep - 1))
+    tokens_on(chips - 1)
+    gate_spread.wait(n_ep - 1)
+    up_spread.wait(n_ep - 1)
+    sweep(lambda far: far < chips - 1, [n_ep - 1])
+    tokens_across(chips - 1)
+    sweep(lambda far: far == chips - 1, range(n_ep))
 
     take_down.wait()
-    rs_order = tp_order[::-1]
     arrivals = {}
-    for position in coming:
-        for copy in coming[position]:
-            copy.wait_send()
+    for line in token_lines:
+        for far in range(1, chips):
+            line.push(far, "wait_send")
+    for line in token_across:
+        for far in range(chips):
+            line.act(far, "wait_send")
 
     def columns_of(c):
-        return pl.ds(c * chunk, chunk)
+        return pl.ds(pl.multiple_of(c * chunk, chunk), chunk)
 
     def down_of(c):
         return jnp.concatenate(
@@ -498,38 +557,79 @@
             preferred_element_type=F32,
         )
 
-    def reduce_send(c, step, started=True):
-        count = n_tp >> (step + 1)
-        arrivals[c, step] = send(
-            tokens.at[pl.ds(count * rows, count * rows), columns_of(c)],
-            landed.at[pl.ds((count - 1) * rows, count * rows), columns_of(c)],
-            rs_send.at[c, step],
-            rs_recv.at[c, step],
-            {"tp": flipped(me_tp, rs_order[step])},
-            started,
-        )
-        return arrivals[c, step]
-
-    def arrived(c, step):
-        count = n_tp >> (step + 1)
-        arrivals[c, step].wait_recv()
-        return landed[pl.ds((count - 1) * rows, count * rows), columns_of(c)].astype(F32)
-
-    def keep(c, value, count):
-        upper = count // 2
-        tokens[pl.ds(upper * rows, upper * rows), columns_of(c)] = value[upper * rows :].astype(BF16)
-        held[pl.ds(0, upper * rows), columns_of(c)] = value[: upper * rows]
-
     def reduce_open(c):
         for offset in range(1, n_ep):
             down_waits[c, offset].wait_recv()
-        tokens[pl.ds(side * rows, side * rows), columns_of(c)] = down_dot(c, side, side).astype(BF16)
-        reduce_send(c, 0)
-        return down_dot(c, 0, side)
-
-    def reduce_kept(c, step):
-        count = n_tp >> (step + 1)
-        return held[pl.ds(0, count * rows), columns_of(c)] + arrived(c, step)
+        upper = pl.ds(chips * rows, chips * rows)
+        tokens[upper, columns_of(c)] = down_dot(c, chips, chips).astype(BF16)
+        arrivals[c] = send(
+            tokens.at[upper, columns_of(c)],
+            landed.at[:, columns_of(c)],
+            rs_send.at[2 * CHUNKS + c, 0],
+            rs_recv.at[2 * CHUNKS + c, 0],
+            sibling,
+        )
+
+    def reduce_pair(c):
+        lower = pl.ds(0, chips * rows)
+        value = down_dot(c, 0, chips)
+        arrivals[c].wait_recv()
+        value = value + landed[:, columns_of(c)].astype(F32)
+        tokens[lower, columns_of(c)] = value.astype(BF16)
+        total[:, columns_of(c)] = sum(
+            jnp.where(chip == b, value[b * rows : (b + 1) * rows], 0.0) for b in range(chips)
+        )
+
+    def passed(flow, c, far, block, place):
+        return pltpu.make_async_remote_copy(
+            src_ref=tokens.at[span_of(block), columns_of(c)],
+            dst_ref=passing.at[span_of(place), columns_of(c)],
+            send_sem=rs_send.at[flow * CHUNKS + c, far],
+            recv_sem=rs_recv.at[flow * CHUNKS + c, far],
+            device_id=flows[flow][1],
+            device_id_type=MESH,
+        )
+
+    def place_of(flow, far, block):
+        return jnp.where(far == 1, chips, block) if flow else block
+
+    def reduce_flow(flow, c):
+        way, _, ahead, behind = flows[flow]
+        going = (c >= 0) & (c < CHUNKS)
+        for far in range(chips - 1, 0, -1):
+            block = chip + way * far
+            source = (span_of(block), columns_of(c))
+
+            if far + 1 < chips:
+
+                @pl.when(going & (ahead >= far) & (behind > 0))
+                def _():
+                    passed(flow, c, far + 1, chip, block).wait_recv()
+                    tokens[source] = (
+                        tokens[source].astype(F32) + passing[source].astype(F32)
+                    ).astype(BF16)
+
+            @pl.when(going & (ahead >= far))
+            def _():
+                passed(flow, c, far, block, place_of(flow, far, block)).start()
+
+        @pl.when(going & (behind > 0))
+        def _():
+            place = place_of(flow, 1, chip)
+            passed(flow, c, 1, chip, place).wait_recv()
+            columns_here = columns_of(c)
+            total[:, columns_here] += passing[span_of(place), columns_here].astype(F32)
+
+    def reduce_gone(c, carry):
+        for flow, (way, _, ahead, _) in enumerate(flows):
+            for far in range(1, chips):
+
+                @pl.when(ahead >= far)
+                def _(flow=flow, far=far, way=way):
+                    block = chip + way * far
+                    passed(flow, c, far, block, block).wait_send()
+
+        return carry
 
     crossed = {}
 
@@ -539,8 +639,8 @@
         crossed[offset] = send(
             share.at[offset, pl.ds(0, 2 * cut)],
             share.at[offset, pl.ds(2 * cut, 2 * cut)],
-            tp_send.at[4, offset],
-            tp_recv.at[4, offset],
+            all_send.at[1, offset],
+            all_recv.at[1, offset],
             {"tp": flipped(me_tp, 1)},
         )
 
@@ -554,35 +654,26 @@
             joined, share[offset], preferred_element_type=F32
         )
 
-    for tick in range(CHUNKS + LAG * (steps - 1)):
-        leaving = []
+    reduce_open(0)
+    for tick in range(CHUNKS + LAG * (chips - 1)):
+        if tick + 1 < CHUNKS:
+            reduce_open(tick + 1)
         if tick < CHUNKS:
-            value = reduce_open(tick)
-            keep(tick, value + arrived(tick, 0), side)
-            leaving.append(reduce_send(tick, 1, False))
-        for step in range(1, steps - 1):
-            c = tick - LAG * step
-            if 0 <= c < CHUNKS:
-                keep(c, reduce_kept(c, step), n_tp >> (step + 1))
-                leaving.append(reduce_send(c, step + 1, False))
-        if leaving:
-            start_by_core(leaving)
-        c = tick - LAG * (steps - 1)
-        if c >= 0:
-            total[:, columns_of(c)] = reduce_kept(c, steps - 1)
+            reduce_pair(tick)
+        for flow, (_, _, _, behind) in enumerate(flows):
+            reduce_flow(flow, tick - LAG * behind)
         if tick == 0:
-            for step in range(1, steps - 1):
-                for position in range(1, 1 << step):
-                    share_wait(position)
-                    share_send(position, step)
-        if tick == SHARE_FIRST:
-            for position in range(1, side):
-                share_wait(position)
+            start_pieces(False)
+        if 0 < tick < chips:
+            share_line.take(tick)
+            if tick + 1 < chips:
+                share_line.push(tick + 1)
+        if tick == chips - 1:
             share_across(0)
             for step in range(len(forth)):
                 for spread in share_spreads:
                     spread.first(step)
-        if tick == SHARE_ON:
+        if tick == chips + 2:
             for spread in share_spreads:
                 spread.forward()
             for offset in forth:
@@ -590,18 +681,24 @@
             for copy in piece_waits:
                 copy.wait_recv()
             project(0)
-
-    for offset in range(1, n_ep):
-        if offset not in crossed:
-            share_across(offset)
-    for offset in range(1, n_ep):
-        project(offset)
+        if tick == max(CHUNKS, chips) + 3:
+            for offset in range(1, n_ep):
+                if offset not in crossed:
+                    share_across(offset)
+            for offset in range(1, n_ep):
+                project(offset)
+            take_mix.wait()
+            mixed[...] = scale_rows(projected[...], mix_gain[...]).astype(BF16)
+
+    for far in range(1, chips):
+        share_line.push(far, "wait_send")
+    lax.fori_loop(0, CHUNKS, reduce_gone, 0)
     for copy in sent:
         copy.wait_send()
 
 
-def finish(projected, total, mix_gain, out_gain, mixer_output, moe_output):
-    mixer_output[...] = scale_rows(projected[...], mix_gain[...]).astype(BF16)
+def finish(mixed, total, out_gain, mixer_output, moe_output):
+    mixer_output[...] = mixed[...]
     moe_output[...] = scale_rows(total[...], out_gain[...]).astype(BF16)
 
 
@@ -618,15 +715,16 @@
     whole = pl.BlockSpec(memory_space=pltpu.VMEM)
     scalar = pl.BlockSpec(memory_space=pltpu.SMEM)
     outside = pl.BlockSpec(memory_space=pl.ANY)
-    steps = (n_tp - 1).bit_length()
+    chips = n_tp // 2
     copies = 6 + CHUNKS
-    projected, total = pl.pallas_call(
+    mixed, total = pl.pallas_call(
         functools.partial(kernel, n_ep, n_tp),
-        out_shape=[jax.ShapeDtypeStruct((rows, width), F32)] * 2,
-        in_specs=[outside] * 3 + [scalar] * 2 + [outside] * 9,
+        out_shape=[jax.ShapeDtypeStruct((rows, width), kind) for kind in (BF16, F32)],
+        in_specs=[outside] * 3 + [scalar] * 2 + [outside] * 10,
         out_specs=[whole, whole],
         scratch_shapes=[
             pltpu.VMEM(queries.shape, BF16),
+            pltpu.VMEM((1, width), F32),
             pltpu.VMEM((1, width), F32),
             pltpu.VMEM((groups, width), BF16),
             pltpu.VMEM((experts, width), BF16),
@@ -635,21 +733,26 @@
             pltpu.VMEM((n_ep, local, width, units), BF16),
             pltpu.VMEM((n_ep, local, width, units), BF16),
             pltpu.VMEM((group_rows, width), BF16),
-            pltpu.VMEM((n_tp, max(8, experts), rows), F32),
+            pltpu.VMEM((n_tp * max(8, experts), rows), F32),
             pltpu.VMEM((WINDOW + group_rows, keys.shape[1]), BF16),
             pltpu.VMEM((WINDOW + group_rows, values.shape[1]), BF16),
             pltpu.VMEM((n_tp, rows, queries.shape[1]), BF16),
             pltpu.VMEM((n_ep, out_weight.shape[0] * n_tp, columns), BF16),
+            pltpu.VMEM((rows, width), F32),
             pltpu.VMEM((group_rows, n_ep * local * units), BF16),
-            pltpu.VMEM((group_rows - rows, width), BF16),
-            pltpu.VMEM((group_rows // 4, width), F32),
+            pltpu.VMEM((chips * rows, width), BF16),
+            pltpu.VMEM((chips * rows + rows, width), BF16),
             pltpu.SemaphoreType.DMA((16,)),
             pltpu.SemaphoreType.DMA((copies, n_ep)),
             pltpu.SemaphoreType.DMA((copies, n_ep)),
-            pltpu.SemaphoreType.DMA((5, max(n_tp, n_ep))),
-            pltpu.SemaphoreType.DMA((5, max(n_tp, n_ep))),
-            pltpu.SemaphoreType.DMA((CHUNKS, steps)),
-            pltpu.SemaphoreType.DMA((CHUNKS, steps)),
+            pltpu.SemaphoreType.DMA((8, chips)),
+            pltpu.SemaphoreType.DMA((8, chips)),
+            pltpu.SemaphoreType.DMA((6, chips)),
+            pltpu.SemaphoreType.DMA((6, chips)),
+            pltpu.SemaphoreType.DMA((2, max(n_tp, n_ep))),
+            pltpu.SemaphoreType.DMA((2, max(n_tp, n_ep))),
+            pltpu.SemaphoreType.DMA((3 * CHUNKS, chips)),
+            pltpu.SemaphoreType.DMA((3 * CHUNKS, chips)),
         ],
         compiler_params=pltpu.CompilerParams(
             collective_id=0, has_side_effects=True, vmem_limit_bytes=67000000
@@ -663,6 +766,7 @@
         out_weight,
         moe_input,
         in_gain[None],
+        mix_gain[None],
         group_router.T,
         expert_router.T,
         routes.T,
@@ -673,9 +777,9 @@
     return pl.pallas_call(
         finish,
         out_shape=[jax.ShapeDtypeStruct((rows, width), BF16)] * 2,
-        in_specs=[whole] * 4,
+        in_specs=[whole] * 3,
         out_specs=[whole] * 2,
-    )(projected, total, mix_gain[None], out_gain[None])
+    )(mixed, total, out_gain[None])
 
 
 def solution(mesh):

time: 107 us -> 104 us (0.972)
  Pallas kernels: 106 us -> 103 us
    pallas_call x1, Pallas kernels: 103 us -> 101 us  [per_device(): pl.pallas_call(functools.partial(kernel, n_ep, n_tp), out_shape=[jax.Shap...]
where the time goes in v2:
time: 104 us
  Pallas kernels  103 us (99%)
    pallas_call x1, Pallas kernels, per_device(): pl.pallas_call(functools.partial(kernel, n_ep, n_tp), out_shape=[jax.Shap...  101 us
    pallas_call x1, Pallas kernels, per_device(): pl.pallas_call(finish, out_shape=[jax.ShapeDtypeStruct((rows, width), BF1...  2.51 us

profile of v2, /device:TPU:1, one launch (start us, length us, event | category | flops | bytes accessed | tf_op | source)
XLA Modules:
  0.0 103.9 jit_solution(12453050190264565255)
XLA Ops:
  0.6 100.8 %shard_map.167 = (bf16[128,2048]{1,0:T(8,128)(2,1)}, f32[128,2048]{1,0:T(8,128)}) custom-call(bf16[1024,128]{1,0:T(8,128)(2,1)} %queries_out.1, bf16[1024,256]{1,0:T(8,128)(2,1)} %keys.1, bf16[1024,256]{1,0:T(8,128)(2,1)} %values.1, f32[2]{0:T(128)} %slopes.1, f32[2]{0:T(128)} %sinks.1, bf16[128,2048]{1,0:T(8,128)(2,1)} %out_weight.1, ...), custom_call_target="tpu_custom_call" | custom-call | tf_op jit(solution)/shard_map/pallas_call | solution.py:720
  101.4 2.5 %shard_map.168 = (bf16[128,2048]{1,0:T(8,128)(2,1)}, bf16[128,2048]{1,0:T(8,128)(2,1)}) custom-call(bf16[128,2048]{1,0:T(8,128)(2,1)} %get-tuple-element.4.mixed, f32[128,2048]{1,0:T(8,128)} %get-tuple-element.5.total, f32[1,2048]{1,0:T(1,128)} %bitcast.10), custom_call_target="tpu_custom_call" | custom-call | tf_op jit(solution)/shard_map/pallas_call | solution.py:777

commit v3 on v2

--- a/solution.py
+++ b/solution.py
@@ -239,6 +239,10 @@
             ),
         ],
     )
+    for copy in take_input:
+        copy.wait()
+    normed = scale_rows(tokens[own_span].astype(F32), in_gain[...]).astype(BF16)
+    tokens[own_span] = normed
     neighbours = sum(jnp.where(ahead > 0, 1, 0) for _, _, ahead, _ in flows)
     pl.semaphore_wait(barrier, len(greeted) + neighbours)
 
@@ -258,10 +262,86 @@
         gate_spread.first(step)
         up_spread.first(step)
 
-    for copy in take_input:
-        copy.wait()
-    normed = scale_rows(tokens[own_span].astype(F32), in_gain[...]).astype(BF16)
-    tokens[own_span] = normed
+    def span_of(block):
+        return pl.ds(pl.multiple_of(block * rows, rows), rows)
+
+    class Line:
+        def __init__(self, number, ref, part=0, parts=1):
+            self.number, self.ref = number, ref
+            self.height = ref.shape[0] // n_tp // parts
+            self.part, self.parts = part, parts
+
+        def at(self, block):
+            start = (block * self.parts + self.part) * self.height
+            return self.ref.at[pl.ds(pl.multiple_of(start, self.height), self.height)]
+
+        def copy(self, flow, far, block, where):
+            number = 2 * self.number + flow
+            return pltpu.make_async_remote_copy(
+                src_ref=self.at(block),
+                dst_ref=self.at(block),
+                send_sem=tp_send.at[number, far],
+                recv_sem=tp_recv.at[number, far],
+                device_id=where,
+                device_id_type=MESH,
+            )
+
+        def push(self, far, act="start"):
+            for flow, (way, following, ahead, behind) in enumerate(flows):
+
+                @pl.when((ahead > 0) & (behind >= far - 1))
+                def _(flow=flow, way=way, following=following):
+                    getattr(self.copy(flow, far, chip - way * (far - 1), following), act)()
+
+        def take(self, far):
+            for flow, (way, following, ahead, behind) in enumerate(flows):
+
+                @pl.when(behind >= far)
+                def _(flow=flow, way=way):
+                    self.copy(flow, far, chip - way * far, sibling).wait_recv()
+
+    class Across:
+        def __init__(self, line):
+            self.line = line
+
+        def copy(self, flow, far, block):
+            number = 2 * self.line.number + flow
+            return pltpu.make_async_remote_copy(
+                src_ref=self.line.at(block),
+                dst_ref=self.line.at(chips + block),
+                send_sem=core_send.at[number, far],
+                recv_sem=core_recv.at[number, far],
+                device_id=sibling,
+                device_id_type=MESH,
+            )
+
+        def act(self, far, what):
+            if far == 0:
+                getattr(self.copy(0, 0, chip), what)()
+                return
+            for flow, (way, _, _, behind) in enumerate(flows):
+
+                @pl.when(behind >= far)
+                def _(flow=flow, way=way):
+                    getattr(self.copy(flow, far, chip - way * far), what)()
+
+    token_lines = [Line(0, tables), Line(1, tokens, 0, 2), Line(2, tokens, 1, 2)]
+    token_across = [Across(line) for line in token_lines]
+
+    def tokens_on(far, chosen=slice(None)):
+        for line in token_lines[chosen]:
+            if far:
+                line.take(far)
+            if far + 1 < chips:
+                line.push(far + 1)
+        for line in token_across[chosen]:
+            line.act(far, "start")
+
+    def tokens_across(far):
+        for line in token_across:
+            line.act(far, "wait_recv")
+
+    tokens_on(0, slice(1, None))
     for copy in take_router:
         copy.wait()
 
@@ -296,86 +376,7 @@
         table = jnp.concatenate([table, jnp.zeros((height - experts, rows), F32)], axis=0)
     tables[pl.ds(pl.multiple_of(chip * height, height), height)] = table
 
-    def span_of(block):
-        return pl.ds(pl.multiple_of(block * rows, rows), rows)
-
-    class Line:
-        def __init__(self, number, ref, part=0, parts=1):
-            self.number, self.ref = number, ref
-            self.height = ref.shape[0] // n_tp // parts
-            self.part, self.parts = part, parts
-
-        def at(self, block):
-            start = (block * self.parts + self.part) * self.height
-            return self.ref.at[pl.ds(pl.multiple_of(start, self.height), self.height)]
-
-        def copy(self, flow, far, block, where):
-            number = 2 * self.number + flow
-            return pltpu.make_async_remote_copy(
-                src_ref=self.at(block),
-                dst_ref=self.at(block),
-                send_sem=tp_send.at[number, far],
-                recv_sem=tp_recv.at[number, far],
-                device_id=where,
-                device_id_type=MESH,
-            )
-
-        def push(self, far, act="start"):
-            for flow, (way, following, ahead, behind) in enumerate(flows):
-
-                @pl.when((ahead > 0) & (behind >= far - 1))
-                def _(flow=flow, way=way, following=following):
-                    getattr(self.copy(flow, far, chip - way * (far - 1), following), act)()
-
-        def take(self, far):
-            for flow, (way, following, ahead, behind) in enumerate(flows):
-
-                @pl.when(behind >= far)
-                def _(flow=flow, way=way):
-                    self.copy(flow, far, chip - way * far, sibling).wait_recv()
-
-    class Across:
-        def __init__(self, line):
-            self.line = line
-
-        def copy(self, flow, far, block):
-            number = 2 * self.line.number + flow
-            return pltpu.make_async_remote_copy(
-                src_ref=self.line.at(block),
-                dst_ref=self.line.at(chips + block),
-                send_sem=core_send.at[number, far],
-                recv_sem=core_recv.at[number, far],
-                device_id=sibling,
-                device_id_type=MESH,
-            )
-
-        def act(self, far, what):
-            if far == 0:
-                getattr(self.copy(0, 0, chip), what)()
-                return
-            for flow, (way, _, _, behind) in enumerate(flows):
-
-                @pl.when(behind >= far)
-                def _(flow=flow, way=way):
-                    getattr(self.copy(flow, far, chip - way * far), what)()
-
-    token_lines = [Line(0, tables), Line(1, tokens, 0, 2), Line(2, tokens, 1, 2)]
-    token_across = [Across(line) for line in token_lines]
-
-    def tokens_on(far):
-        for line in token_lines:
-            if far:
-                line.take(far)
-            if far + 1 < chips:
-                line.push(far + 1)
-        for line in token_across:
-            line.act(far, "start")
-
-    def tokens_across(far):
-        for line in token_across:
-            line.act(far, "wait_recv")
-
-    tokens_on(0)
+    tokens_on(0, slice(0, 1))
 
     def to_all(number, source_of, target_of):
         waits = []

time: 104 us -> 104 us (level)
  no operation moved by 1% of the time
where the time goes in v3:
time: 104 us
  Pallas kernels  103 us (99%)
    pallas_call x1, Pallas kernels, per_device(): pl.pallas_call(functools.partial(kernel, n_ep, n_tp), out_shape=[jax.Shap...  101 us
    pallas_call x1, Pallas kernels, per_device(): pl.pallas_call(finish, out_shape=[jax.ShapeDtypeStruct((rows, width), BF1...  2.51 us

profile of v3, /device:TPU:1, one launch (start us, length us, event | category | flops | bytes accessed | tf_op | source)
XLA Modules:
  0.0 103.9 jit_solution(7222751376729705485)
XLA Ops:
  0.6 100.8 %shard_map.167 = (bf16[128,2048]{1,0:T(8,128)(2,1)}, f32[128,2048]{1,0:T(8,128)}) custom-call(bf16[1024,128]{1,0:T(8,128)(2,1)} %queries_out.1, bf16[1024,256]{1,0:T(8,128)(2,1)} %keys.1, bf16[1024,256]{1,0:T(8,128)(2,1)} %values.1, f32[2]{0:T(128)} %slopes.1, f32[2]{0:T(128)} %sinks.1, bf16[128,2048]{1,0:T(8,128)(2,1)} %out_weight.1, ...), custom_call_target="tpu_custom_call" | custom-call | tf_op jit(solution)/shard_map/pallas_call | solution.py:721
  101.4 2.5 %shard_map.168 = (bf16[128,2048]{1,0:T(8,128)(2,1)}, bf16[128,2048]{1,0:T(8,128)(2,1)}) custom-call(bf16[128,2048]{1,0:T(8,128)(2,1)} %get-tuple-element.4.mixed, f32[128,2048]{1,0:T(8,128)} %get-tuple-element.5.total, f32[1,2048]{1,0:T(1,128)} %bitcast.10), custom_call_target="tpu_custom_call" | custom-call | tf_op jit(solution)/shard_map/pallas_call | solution.py:778
